TPU v7x, 128 devices: a whole 4x4x4 slice. The times are simulated.
128 devices in a mesh: ep: 16 (over z, x), tp: 8 (over y, core).
Axes of the slice: x: 4, y: 4, z: 4, core: 2. Of those that a mesh axis runs over, the one named last changes fastest.
Arguments:
- residual: bfloat16 [2048, 2048], P('ep', 'tp'), may hold values from -61 to 61
- in_gain: float32 [2048], replicated, may hold values from 0.1 to 1.9
- in_weight: bfloat16 [2048, 1024], P(None, 'tp'), may hold values from -0.125 to 0.125
- state: float32 [2, 2048, 4096], P(None, 'ep', 'tp'), may hold values from -3 to 3
- decay_rate: float32 [64, 64], P('tp'), may hold values from 0.1 to 1
- frequency: float32 [64, 64], P('tp'), may hold values from 0 to 200
- log_step: float32 [64], P('tp'), may hold values from -3 to -0.7
- in_coef: float32 [2, 64, 64, 16], P(None, 'tp'), may hold values from -1 to 1
- out_coef: float32 [2, 64, 16, 64], P(None, 'tp'), may hold values from -0.75 to 0.75
- skip_gain: float32 [1024], P('tp'), may hold values from -3 to 3
- out_weight: bfloat16 [1024, 2048], replicated, may hold values from -0.1875 to 0.1875
- mid_gain: float32 [2048], replicated, may hold values from 0.1 to 1.9
- gate_vector: bfloat16 [2048], replicated, may hold values from -0.125 to 0.125
- routes: int32 [2048, 4], P('ep'), may hold values from 0 to 127, all different within a row; in each aligned block of 128 rows (0 to 127, 128 to 255, ...) at most 8 rows name the same one
- route_weight: float32 [2048, 4], P('ep'), may hold values from 0.1 to 1
- expert_gate: bfloat16 [128, 2048, 512], P(('ep', 'tp')), may hold values from -0.125 to 0.125
- expert_up: bfloat16 [128, 2048, 512], P(('ep', 'tp')), may hold values from -0.125 to 0.125
- expert_down: bfloat16 [128, 512, 2048], P(('ep', 'tp')), may hold values from -0.25 to 0.25
- shared_gate: bfloat16 [2048, 4096], P(None, 'ep'), may hold values from -0.125 to 0.125
- shared_up: bfloat16 [2048, 4096], P(None, 'ep'), may hold values from -0.125 to 0.125
- shared_down: bfloat16 [4096, 2048], P('ep'), may hold values from -0.09375 to 0.09375
Outputs:
- layer_out: bfloat16 [2048, 2048], P(('ep', 'tp'))
- new_state: float32 [2, 2048, 4096], P(None, 'ep', 'tp')
Inputs may be any that keep to these rules, and one draw needn't show every extreme that they name: `routes`: each row names 4 different experts. Among the rows of one index of ep no expert is named more than 8 times, a bound that some block reaches.
All inputs are finite; a program needn't handle non-finite values.
Results may differ from a plain program's by a relative error of at most 0.0085.
Values may be sent and summed in bfloat16 or wider, within the bound.
No kernel may reach another device: no remote copies, remote signals or barrier semaphores. Data moves between devices by JAX's collectives and lax.ppermute only.
A program may use at most 128 MiB of HBM per device.

v0:
```python
import jax
import jax.numpy as jnp
from jax import lax
from jax.sharding import PartitionSpec as P

norm_eps = 1e-05
routed_scale = 2.5


def laid_out(blocks, dim):
    dims = list(blocks.shape[1:])
    dims[dim] *= blocks.shape[0]
    return jnp.moveaxis(blocks, 0, dim).reshape(dims)


def from_everyone(array, axis):
    length = lax.axis_size(axis)
    return lax.all_to_all(
        jnp.broadcast_to(array[None], (length, *array.shape)), axis, 0, 0, tiled=True
    )


def gather_directly(array, axis, dim):
    return laid_out(from_everyone(array, axis), dim)


def in_one_piece(arrays, axis, split_dim, concat_dim, along):
    both = jnp.concatenate(arrays, axis=along)
    result, at, finished = (
        lax.all_to_all(both, axis, split_axis=split_dim, concat_axis=concat_dim, tiled=True),
        0,
        [],
    )
    for a in arrays:
        finished.append(lax.slice_in_dim(result, at, at + a.shape[along], axis=along))
        at += a.shape[along]
    return tuple(finished)


def in_blocks(array, dim, length):
    before, after = (array.shape[:dim], array.shape[dim + 1 :])
    return jnp.moveaxis(array.reshape(*before, length, -1, *after), dim, 0)


def sent_and_summed(array, axis, dim):
    length = lax.axis_size(axis)
    blocks = lax.all_to_all(in_blocks(array, dim, length), axis, 0, 0, tiled=True)
    return jnp.sum(blocks.astype(jnp.float32), axis=0)


def layer_norm(values, gain_vec):
    row_mean = jnp.mean(values, axis=-1, keepdims=True)
    row_square = jnp.mean(values * values, axis=-1, keepdims=True)
    return (values - row_mean) * lax.rsqrt(row_square - row_mean * row_mean + norm_eps) * gain_vec


def coefficients(decay_rate, frequency, log_step, in_coef):
    time_step = jnp.exp(log_step)[:, None]
    real_rate = -decay_rate
    magnitude = jnp.exp(real_rate * time_step)
    keep_re = magnitude * jnp.cos(frequency * time_step)
    keep_im = magnitude * jnp.sin(frequency * time_step)
    denominator = real_rate * real_rate + frequency * frequency
    factor_re = ((keep_re - 1.0) * real_rate + keep_im * frequency) / denominator
    factor_im = (keep_im * real_rate - (keep_re - 1.0) * frequency) / denominator
    push_re = factor_re[..., None] * in_coef[0] - factor_im[..., None] * in_coef[1]
    push_im = factor_re[..., None] * in_coef[1] + factor_im[..., None] * in_coef[0]
    return (keep_re, keep_im, push_re, push_im)


def mixer_step(
    normed, in_weight, state, decay_rate, frequency, log_step, in_coef, out_coef, skip_gain
):
    row_count = normed.shape[0]
    group_count, state_count = decay_rate.shape
    keep_re, keep_im, push_re, push_im = coefficients(decay_rate, frequency, log_step, in_coef)
    drive = jnp.dot(normed, in_weight, preferred_element_type=jnp.float32).astype(jnp.bfloat16)
    drive_f = drive.astype(jnp.float32).reshape(row_count, group_count, -1)
    input_re = jnp.einsum("tgh,gph->tgp", drive_f, push_re)
    input_im = jnp.einsum("tgh,gph->tgp", drive_f, push_im)
    old_re = state[0].reshape(row_count, group_count, state_count)
    old_im = state[1].reshape(row_count, group_count, state_count)
    new_re = keep_re * old_re - keep_im * old_im + input_re
    new_im = keep_re * old_im + keep_im * old_re + input_im
    read_out = jnp.einsum("ghp,tgp->tgh", out_coef[0], new_re) - jnp.einsum(
        "ghp,tgp->tgh", out_coef[1], new_im
    )
    read_out = read_out.reshape(row_count, -1) + skip_gain * drive_f.reshape(row_count, -1)
    mixed_rows = jax.nn.gelu(read_out, approximate=True).astype(jnp.bfloat16)
    updated = jnp.stack([new_re.reshape(row_count, -1), new_im.reshape(row_count, -1)])
    return (mixed_rows, updated)


def route_slots(routes, experts):
    flat_routes = routes.reshape(-1)
    onehot = (flat_routes[:, None] == jnp.arange(experts, dtype=jnp.int32)[None, :]).astype(
        jnp.int32
    )
    before = jnp.cumsum(onehot, axis=0) - onehot
    return jnp.sum(before * onehot, axis=1).reshape(routes.shape)


def expert_block(row_block, gate_weight, up_weight, down_weight):
    gate_part = jnp.dot(row_block, gate_weight, preferred_element_type=jnp.float32)
    up_part = jnp.dot(row_block, up_weight, preferred_element_type=jnp.float32)
    hidden = (jax.nn.silu(gate_part) * up_part).astype(jnp.bfloat16)
    return jnp.dot(hidden, down_weight, preferred_element_type=jnp.float32).astype(jnp.bfloat16)


def per_device(
    residual,
    in_gain,
    in_weight,
    state,
    decay_rate,
    frequency,
    log_step,
    in_coef,
    out_coef,
    skip_gain,
    out_weight,
    mid_gain,
    gate_vector,
    routes,
    route_weight,
    expert_gate,
    expert_up,
    expert_down,
    shared_gate,
    shared_up,
    shared_down,
):
    tp_count = lax.axis_size("tp")
    ep_count = lax.axis_size("ep")
    tp_place = lax.axis_index("tp")
    seq_rows, feat_part = residual.shape
    width = feat_part * tp_count
    full_resid = gather_directly(residual, "tp", 1)
    normed = layer_norm(full_resid.astype(jnp.float32), in_gain).astype(jnp.bfloat16)
    mixed_part, new_state = mixer_step(
        normed, in_weight, state, decay_rate, frequency, log_step, in_coef, out_coef, skip_gain
    )
    mixed_rows = lax.all_gather(mixed_part, "tp", axis=1, tiled=True)
    after_mix = full_resid.astype(jnp.float32) + jnp.dot(
        mixed_rows, out_weight, preferred_element_type=jnp.float32
    )
    normed_mid = layer_norm(after_mix, mid_gain).astype(jnp.bfloat16)
    per_dev = seq_rows // tp_count
    own_mid = lax.dynamic_slice_in_dim(normed_mid, tp_place * per_dev, per_dev, 0)
    own_after = lax.dynamic_slice_in_dim(after_mix, tp_place * per_dev, per_dev, 0)
    experts = ep_count * tp_count
    top_count = routes.shape[1]
    capacity = max(2, 2 * seq_rows * top_count // experts)
    slot_rank = route_slots(routes, experts)
    dest_tp = routes % tp_count
    dest_ep = routes // tp_count
    is_mine = dest_tp == tp_place
    slot_place = dest_ep * capacity + slot_rank
    slot_total = ep_count * capacity
    matches = (
        slot_place.reshape(-1)[None, :] == jnp.arange(slot_total, dtype=jnp.int32)[:, None]
    ) & is_mine.reshape(-1)[None, :]
    token_ids = jnp.repeat(jnp.arange(seq_rows, dtype=jnp.int32), top_count)
    slot_token = jnp.sum(jnp.where(matches, token_ids[None, :], 0), axis=1)
    outgoing = normed_mid[slot_token].reshape(ep_count, capacity, width)
    copies = jnp.broadcast_to(own_mid[None], (ep_count, per_dev, width))
    got_slots, got_rows = in_one_piece((outgoing, copies), "ep", 0, 0, 1)
    flat_rows = got_slots.reshape(-1, width)
    result = expert_block(flat_rows, expert_gate[0], expert_up[0], expert_down[0])
    computed = result.reshape(got_slots.shape)
    returned = lax.all_to_all(computed, "ep", split_axis=0, concat_axis=0, tiled=True)
    piece = got_rows.reshape(-1, width)
    gate_part = jnp.dot(piece, shared_gate, preferred_element_type=jnp.float32)
    up_part = jnp.dot(piece, shared_up, preferred_element_type=jnp.float32)
    shared_hidden = (jax.nn.silu(gate_part) * up_part).astype(jnp.bfloat16)
    partial_rows = jnp.dot(shared_hidden, shared_down, preferred_element_type=jnp.float32)
    partial_back = lax.all_to_all(
        partial_rows.reshape(ep_count, per_dev, width).astype(jnp.bfloat16),
        "ep",
        split_axis=0,
        concat_axis=0,
        tiled=True,
    ).astype(jnp.float32)
    shared = jnp.sum(partial_back, axis=0)
    flat_back = returned.reshape(slot_total, width)
    weights = route_weight / jnp.sum(route_weight, axis=-1, keepdims=True) * routed_scale
    picked = flat_back[jnp.where(is_mine, slot_place, 0)].astype(jnp.float32)
    routed_part = jnp.sum(jnp.where(is_mine, weights, 0.0)[..., None] * picked, axis=1)
    routed = sent_and_summed(routed_part.astype(jnp.bfloat16), "tp", 0)
    gate_value = jax.nn.sigmoid(jnp.dot(own_mid, gate_vector, preferred_element_type=jnp.float32))
    layer_out = (own_after + routed + gate_value[:, None] * shared).astype(jnp.bfloat16)
    return (layer_out, new_state)


def solution(mesh):
    return jax.shard_map(
        per_device,
        mesh=mesh,
        in_specs=(
            P("ep", "tp"),
            P(),
            P(None, "tp"),
            P(None, "ep", "tp"),
            P("tp", None),
            P("tp", None),
            P("tp"),
            P(None, "tp", None, None),
            P(None, "tp", None, None),
            P("tp"),
            P(),
            P(),
            P(),
            P("ep", None),
            P("ep", None),
            P(("ep", "tp"), None, None),
            P(("ep", "tp"), None, None),
            P(("ep", "tp"), None, None),
            P(None, "ep"),
            P(None, "ep"),
            P("ep", None),
        ),
        out_specs=(P(("ep", "tp"), None), P(None, "ep", "tp")),
        check_vma=False,
    )
```

profile of v0, /device:TPU:0, one launch (start us, length us, event | category | flops | bytes accessed | tf_op | source)
XLA Modules:
  0.0 138.5 jit_solution(16512454888797237247)
XLA Ops:
  0.7 1.8 %broadcast_in_dim.22 = bf16[8,128,256]{2,1,0:T(8,128)(2,1)} broadcast(bf16[128,256]{1,0:T(8,128)(2,1)} %param.21), dimensions={1,2} | broadcast | bytes 589824 | tf_op jit(solution)/shard_map/broadcast_in_dim | solution.py:19
  2.5 4.6 %all-to-all-start = ((bf16[8,128,256]{2,1,0:T(8,128)(2,1)}), bf16[8,128,256]{2,1,0:T(8,128)(2,1)S(1)}, u32[]{:S(2)}, u32[]{:S(2)}) async-start(bf16[8,128,256]{2,1,0:T(8,128)(2,1)} %broadcast_in_dim.22), calls=%async_computation | async-start | bytes 1048576 | tf_op jit(solution)/shard_map/all_to_all | solution.py:18
  7.1 0.8 copy.88
  7.8 0.1 eq.54
  8.0 0.1 eq.50
  8.1 0.7 exp.17
  8.7 0.7 reduce_sum.94
  9.4 0.7 multiply_select_fusion
  10.1 0.1 copy.94
  10.3 0.1 and.23
  10.4 0.1 copy.90
  10.6 0.1 broadcast_in_dim.25
  10.7 0.2 fusion.37
  11.0 0.2 fusion.26
  11.2 0.1 reshape.121
  11.4 0.1 copy.93
  11.5 0.1 eq.58
  11.6 1.1 fusion.78
  12.7 0.1 copy.85
  12.8 0.1 copy.86
  13.0 0.1 select_reduce_fusion
  13.2 0.1 add_divide_fusion
  13.3 4.1 %all-to-all-done = bf16[8,128,256]{2,1,0:T(8,128)(2,1)S(1)} async-done(((bf16[8,128,256]{2,1,0:T(8,128)(2,1)}), bf16[8,128,256]{2,1,0:T(8,128)(2,1)S(1)}, u32[]{:S(2)}, u32[]{:S(2)}) %all-to-all-start) | async-done | bytes 524320 | tf_op jit(solution)/shard_map/all_to_all | solution.py:18
  17.6 0.2 convert_reduce_fusion.1
  17.8 0.6 copy-done.7
  18.4 0.4 convolution_convert_fusion.2
  18.9 0.3 fusion.9
  19.2 0.3 fusion.10
  19.5 0.1 fusion.52
  19.6 0.1 convolution_subtract_fusion
  19.8 0.1 fusion.50
  19.9 12.8 %all_gather.3 = bf16[128,1024]{0,1:T(8,128)(2,1)S(1)} all-gather(bf16[128,128]{0,1:T(8,128)(2,1)S(1)} %fusion.50), channel_id=1, replica_groups=mesh['ep'=16,'tp'=8] {'tp'}, dimensions={1}, use_global_device_ids=true | all-gather | bytes 294912 | tf_op jit(solution)/shard_map/all_gather | solution.py:143
  32.7 0.8 fusion.75
  33.6 1.0 copy-done.2
  34.6 0.2 multiply_convert_fusion
  34.8 0.9 gather_fusion
  35.8 0.1 broadcast_in_dim.32
  35.9 0.2 pad_maximum_fusion
  36.1 31.1 %all_to_all.25 = bf16[16,24,2048]{2,1,0:T(8,128)(2,1)S(1)} all-to-all(bf16[16,24,2048]{2,1,0:T(8,128)(2,1)S(1)} %pad_maximum_fusion), channel_id=1, replica_groups=mesh['ep'=16,'tp'=8] {'ep'}, dimensions={0} | all-to-all | bytes 3145728 | tf_op jit(solution)/shard_map/all_to_all | solution.py:30
  67.1 1.2 copy-done.1
  68.3 0.4 fusion.4
  68.8 3.4 %fusion = bf16[16,8,2048]{2,1,0:T(8,128)(2,1)} fusion(bf16[1,512,2048]{2,1,0:T(8,128)(2,1)S(1)} %copy-done, bf16[1,2048,512]{2,1,0:T(8,128)(2,1)} %param.37, bf16[16,24,2048]{2,1,0:T(8,128)(2,1)} %copy-done.1, f32[128,512]{1,0:T(8,128)S(1)} %fusion.4), kind=kOutput, calls=%fused_computation.6 | convolution fusion | flops 537526272 | bytes 5505024 | tf_op jit(solution)/shard_map/dot_general | solution.py:107
  72.2 3.6 %all-to-all-start.2 = ((bf16[16,8,2048]{2,1,0:T(8,128)(2,1)}), bf16[16,8,2048]{2,1,0:T(8,128)(2,1)S(1)}, u32[]{:S(2)}, u32[]{:S(2)}) async-start(bf16[16,8,2048]{2,1,0:T(8,128)(2,1)} %fusion), calls=%async_computation.2 | async-start | bytes 1048576 | tf_op jit(solution)/shard_map/all_to_all | solution.py:171
  75.7 0.1 copy.87
  75.9 0.1 copy.95
  76.0 0.1 reshape.138
  76.1 2.3 %slice.48 = bf16[16,16,2048]{2,1,0:T(8,128)(2,1)} slice(bf16[16,24,2048]{2,1,0:T(8,128)(2,1)} %copy-done.1), slice={[0:16], [8:24], [0:2048]} | slice | bytes 2097152 | tf_op jit(solution)/shard_map/slice | solution.py:35
  78.4 8.2 %all-to-all-done.2 = bf16[16,8,2048]{2,1,0:T(8,128)(2,1)S(1)} async-done(((bf16[16,8,2048]{2,1,0:T(8,128)(2,1)}), bf16[16,8,2048]{2,1,0:T(8,128)(2,1)S(1)}, u32[]{:S(2)}, u32[]{:S(2)}) %all-to-all-start.2) | async-done | bytes 524320 | tf_op jit(solution)/shard_map/all_to_all | solution.py:171
  86.6 3.3 %gather_fusion.1 = bf16[512,2048]{1,0:T(8,128)(2,1)} fusion(bf16[128,2048]{1,0:T(8,128)(2,1)S(1)} %bitcast.115, s32[1024]{0:T(1024)S(1)} %pad_clamp_fusion), kind=kCustom, calls=%fused_computation.1 | custom fusion | bytes 4196352 | tf_op jit(solution)/shard_map/gather | solution.py:187
  89.9 4.8 %reshape.146 = f32[128,4,2048]{2,1,0:T(4,128)} reshape(bf16[512,2048]{1,0:T(8,128)(2,1)} %gather_fusion.1) | data formatting | bytes 6291456 | tf_op jit(solution)/shard_map/convert_element_type | solution.py:187
  94.7 6.3 %multiply_reduce_fusion = bf16[128,2048]{1,0:T(8,128)(2,1)} fusion(f32[128,4,2048]{2,1,0:T(4,128)} %reshape.146, f32[128,4]{1,0:T(8,128)S(1)} %copy.87), kind=kLoop, calls=%fused_computation.2 | loop fusion | flops 1835008 | bytes 4720640 | tf_op jit(solution)/shard_map/reduce_sum | solution.py:188
  100.9 4.1 %all-to-all-start.3 = ((bf16[8,16,2048]{2,1,0:T(8,128)(2,1)}), bf16[8,16,2048]{2,1,0:T(8,128)(2,1)}, u32[]{:S(2)}, u32[]{:S(2)}) async-start(bf16[8,16,2048]{2,1,0:T(8,128)(2,1)} %bitcast.126), calls=%async_computation.3 | async-start | bytes 1048576 | tf_op jit(solution)/shard_map/all_to_all | solution.py:47
  105.1 2.4 %fusion.79 = f32[256,256]{1,0:T(8,128)} fusion(bf16[256,2048]{1,0:T(8,128)(2,1)S(1)} %bitcast.118, bf16[2048,256]{1,0:T(8,128)(2,1)} %param.39), kind=kOutput, calls=%fused_computation.129 | convolution fusion | flops 268435456 | bytes 2359296 | tf_op jit(solution)/shard_map/dot_general | solution.py:173
  107.5 3.9 %convolution_convert_fusion = bf16[256,2048]{1,0:T(8,128)(2,1)} fusion(bf16[256,2048]{1,0:T(8,128)(2,1)} %param.41, bf16[256,2048]{1,0:T(8,128)(2,1)S(1)} %bitcast.119, bf16[2048,256]{1,0:T(8,128)(2,1)} %param.40, f32[256,256]{1,0:T(8,128)} %fusion.79), kind=kOutput, calls=%fused_computation.3 | convolution fusion | flops 537788416 | bytes 4456448 | tf_op jit(solution)/shard_map/dot_general | solution.py:176
  111.4 4.0 %all-to-all-done.3 = bf16[8,16,2048]{2,1,0:T(8,128)(2,1)} async-done(((bf16[8,16,2048]{2,1,0:T(8,128)(2,1)}), bf16[8,16,2048]{2,1,0:T(8,128)(2,1)}, u32[]{:S(2)}, u32[]{:S(2)}) %all-to-all-start.3) | async-done | bytes 524320 | tf_op jit(solution)/shard_map/all_to_all | solution.py:47
  115.4 3.7 %all-to-all-start.4 = ((bf16[16,16,2048]{2,1,0:T(8,128)(2,1)}), bf16[16,16,2048]{2,1,0:T(8,128)(2,1)S(1)}, u32[]{:S(2)}, u32[]{:S(2)}) async-start(bf16[16,16,2048]{2,1,0:T(8,128)(2,1)} %bitcast.129), calls=%async_computation.4 | async-start | bytes 2097152 | tf_op jit(solution)/shard_map/all_to_all | solution.py:177
  119.1 1.8 %copy.97 = f32[1,128,512]{2,1,0:T(8,128)} copy(f32[1,128,512]{1,2,0:T(8,128)} %bitcast.125) | data formatting | bytes 524288 | tf_op jit(solution)/shard_map/stack;reshape | solution.py:90
  120.9 0.8 copy.96
  121.7 1.9 %pad_maximum_fusion.1 = f32[2,128,512]{2,1,0:T(8,128)} fusion(f32[1,128,512]{2,1,0:T(8,128)} %copy.97, f32[1,128,512]{2,1,0:T(8,128)} %copy.96), kind=kLoop, calls=%fused_computation.38 | loop fusion | flops 131072 | bytes 1048576 | tf_op jit(solution)/shard_map/stack | solution.py:90
  123.6 0.1 fusion.18
  123.7 1.1 convert_reduce_fusion.2
  124.9 11.8 %all-to-all-done.4 = bf16[16,16,2048]{2,1,0:T(8,128)(2,1)S(1)} async-done(((bf16[16,16,2048]{2,1,0:T(8,128)(2,1)}), bf16[16,16,2048]{2,1,0:T(8,128)(2,1)S(1)}, u32[]{:S(2)}, u32[]{:S(2)}) %all-to-all-start.4) | async-done | bytes 1048608 | tf_op jit(solution)/shard_map/all_to_all | solution.py:177
  136.7 0.1 convert_reduce_fusion
  136.8 1.6 %add_convert_fusion = bf16[16,2048]{1,0:T(8,128)(2,1)} fusion(f32[16,2048]{1,0:T(8,128)S(1)} %convert_reduce_fusion, f32[16,2048]{1,0:T(8,128)S(1)} %convert_reduce_fusion.2, f32[128,2048]{1,0:T(8,128)} %copy-done.2, s32[]{:T(128)S(6)} %select_n.41, f32[16]{0:T(128)S(1)} %fusion.18), kind=kLoop, calls=%fused_computation.62 | loop fusion | flops 131072 | bytes 458820 | tf_op jit(solution)/shard_map/convert_element_type | solution.py:191
  (49 shorter events, 0.5 us)
Async XLA Ops:
  0.6 68.1 %copy-start = (bf16[1,512,2048]{2,1,0:T(8,128)(2,1)S(1)}, bf16[1,512,2048]{2,1,0:T(8,128)(2,1)}, u32[]{:S(2)}) copy-start(bf16[1,512,2048]{2,1,0:T(8,128)(2,1)} %param.38) | copy-start | bytes 6291460
  0.6 10.7 %copy-start.10 = (s32[128,4]{0,1:T(4,128)S(1)}, s32[128,4]{0,1:T(4,128)}, u32[]{:S(2)}) copy-start(s32[128,4]{0,1:T(4,128)} %param.34) | copy-start | bytes 6148
  2.5 14.9 %all-to-all-start = ((bf16[8,128,256]{2,1,0:T(8,128)(2,1)}), bf16[8,128,256]{2,1,0:T(8,128)(2,1)S(1)}, u32[]{:S(2)}, u32[]{:S(2)}) async-start(bf16[8,128,256]{2,1,0:T(8,128)(2,1)} %broadcast_in_dim.22), calls=%async_computation | async-start | bytes 1048576 | tf_op jit(solution)/shard_map/all_to_all | solution.py:18
  10.5 2.6 %copy-start.13 = (f32[8,64]{1,0:T(8,128)S(1)}, f32[8,64]{1,0:T(8,128)}, u32[]{:S(2)}) copy-start(f32[8,64]{1,0:T(8,128)} %param.26) | copy-start | bytes 6148
  10.5 2.6 %copy-start.14 = (f32[8,64]{1,0:T(8,128)S(1)}, f32[8,64]{1,0:T(8,128)}, u32[]{:S(2)}) copy-start(f32[8,64]{1,0:T(8,128)} %param.25) | copy-start | bytes 6148
  13.3 4.6 %copy-start.11 = (f32[2048]{0:T(1024)S(1)}, f32[2048]{0:T(1024)}, u32[]{:S(2)}) copy-start(f32[2048]{0:T(1024)} %param.22) | copy-start | bytes 24580
  17.4 1.0 copy-start.7
  17.5 1.4 copy-start.8
  17.6 1.9 %copy-start.9 = (f32[2,8,16,64]{3,2,1,0:T(8,128)S(1)}, f32[2,8,16,64]{3,2,1,0:T(8,128)}, u32[]{:S(2)}) copy-start(f32[2,8,16,64]{3,2,1,0:T(8,128)} %param.29) | copy-start | bytes 196612
  18.4 1.4 copy-start.16
  18.4 14.3 %copy-start.3 = (bf16[1024,2048]{1,0:T(8,128)(2,1)S(1)}, bf16[1024,2048]{1,0:T(8,128)(2,1)}, u32[]{:S(2)}) copy-start(bf16[1024,2048]{1,0:T(8,128)(2,1)} %param.31) | copy-start | bytes 12582916
  19.2 14.4 %copy-start.5 = (f32[128,8,64]{0,2,1:T(8,128)}, f32[128,8,64]{0,2,1:T(8,128)S(1)}, u32[]{:S(2)}) copy-start(f32[128,8,64]{0,2,1:T(8,128)S(1)} %fusion.9) | copy-start | bytes 786436
  32.7 1.9 %copy-start.12 = (f32[2048]{0:T(1024)S(1)}, f32[2048]{0:T(1024)}, u32[]{:S(2)}) copy-start(f32[2048]{0:T(1024)} %param.32) | copy-start | bytes 24580
  33.6 1.0 copy-start.2
  36.0 32.3 %copy-start.6 = (bf16[1,2048,512]{2,1,0:T(8,128)(2,1)S(1)}, bf16[1,2048,512]{2,1,0:T(8,128)(2,1)}, u32[]{:S(2)}) copy-start(bf16[1,2048,512]{2,1,0:T(8,128)(2,1)} %param.36) | copy-start | bytes 6291460
  67.1 1.2 copy-start.1
  72.2 14.4 %all-to-all-start.2 = ((bf16[16,8,2048]{2,1,0:T(8,128)(2,1)}), bf16[16,8,2048]{2,1,0:T(8,128)(2,1)S(1)}, u32[]{:S(2)}, u32[]{:S(2)}) async-start(bf16[16,8,2048]{2,1,0:T(8,128)(2,1)} %fusion), calls=%async_computation.2 | async-start | bytes 1048576 | tf_op jit(solution)/shard_map/all_to_all | solution.py:171
  94.7 10.4 %copy-start.4 = (bf16[16,16,2048]{2,1,0:T(8,128)(2,1)S(1)}, bf16[16,16,2048]{2,1,0:T(8,128)(2,1)}, u32[]{:S(2)}) copy-start(bf16[16,16,2048]{2,1,0:T(8,128)(2,1)} %slice.48) | copy-start | bytes 3145732
  100.9 14.5 %all-to-all-start.3 = ((bf16[8,16,2048]{2,1,0:T(8,128)(2,1)}), bf16[8,16,2048]{2,1,0:T(8,128)(2,1)}, u32[]{:S(2)}, u32[]{:S(2)}) async-start(bf16[8,16,2048]{2,1,0:T(8,128)(2,1)} %bitcast.126), calls=%async_computation.3 | async-start | bytes 1048576 | tf_op jit(solution)/shard_map/all_to_all | solution.py:47
  111.4 7.7 %copy-start.15 = (bf16[2048]{0:T(1024)(128)(2,1)S(1)}, bf16[2048]{0:T(1024)(128)(2,1)}, u32[]{:S(2)}) copy-start(bf16[2048]{0:T(1024)(128)(2,1)} %param.33) | copy-start | bytes 12292
  115.4 21.3 %all-to-all-start.4 = ((bf16[16,16,2048]{2,1,0:T(8,128)(2,1)}), bf16[16,16,2048]{2,1,0:T(8,128)(2,1)S(1)}, u32[]{:S(2)}, u32[]{:S(2)}) async-start(bf16[16,16,2048]{2,1,0:T(8,128)(2,1)} %bitcast.129), calls=%async_computation.4 | async-start | bytes 2097152 | tf_op jit(solution)/shard_map/all_to_all | solution.py:177
where the time goes:
time: 139 us; the launch traced here: 138 us
  blocking collectives  43.9 us (32%)
  waiting for transfers between devices  28.1 us (20%)
  local copies, waits for them, and re-layouts  23 us (17%)
  starting transfers between devices  16 us (12%)
  other arithmetic  14.1 us (10%)
  matrix products  12.4 us (9%)
    all_to_all x1, blocking collectives, in_one_piece(): lax.all_to_all(both, axis, split_axis=split_dim, concat_axis=concat_dim,...  31.1 us
    all_gather x1, blocking collectives, per_device(): mixed_rows = lax.all_gather(mixed_part, 'tp', axis=1, tiled=True)  12.8 us
    all_to_all x1, waiting for transfers between devices, per_device(): lax.all_to_all(partial_rows.reshape(ep_count, per_dev, width).astype(jnp....  11.8 us
    all_to_all x1, waiting for transfers between devices, per_device(): lax.all_to_all(computed, 'ep', split_axis=0, concat_axis=0, tiled=True)  8.19 us
    reduce_sum x1, other arithmetic, per_device(): jnp.sum(jnp.where(is_mine, weights, 0.0)[..., None] * picked, axis=1)  6.28 us
    convert_element_type x1, local copies, waits for them, and re-layouts, per_device(): picked = flat_back[jnp.where(is_mine, slot_place, 0)].astype(jnp.float32)  4.75 us
    all_to_all x1, starting transfers between devices, from_everyone(): lax.all_to_all(jnp.broadcast_to(array[None], (length, *array.shape)), axi...  4.58 us
    all_to_all x1, starting transfers between devices, sent_and_summed(): lax.all_to_all(in_blocks(array, dim, length), axis, 0, 0, tiled=True)  4.14 us
  transfers between devices with their start and end apart: 4, of which 4 were waited for; matrix products, arithmetic and copies ran while one was open for 15% of the time, Pallas kernels for 0%

commit v1 on v0

--- a/solution.py
+++ b/solution.py
@@ -140,7 +140,9 @@
     mixed_part, new_state = mixer_step(
         normed, in_weight, state, decay_rate, frequency, log_step, in_coef, out_coef, skip_gain
     )
-    mixed_rows = lax.all_gather(mixed_part, "tp", axis=1, tiled=True)
+    mixed_rows = jnp.concatenate(
+        lax.all_to_all(jnp.stack([mixed_part] * lax.axis_size("tp")), "tp", 0, 0), axis=1
+    )
     after_mix = full_resid.astype(jnp.float32) + jnp.dot(
         mixed_rows, out_weight, preferred_element_type=jnp.float32
     )

time: 139 us -> 141 us (1.014)
  blocking collectives: 43.9 us -> 30.2 us
  waiting for transfers between devices: 28.1 us -> 35.2 us
  starting transfers between devices: 16 us -> 19.5 us
  local copies, waits for them, and re-layouts: 23 us -> 26.3 us
    all_gather x1 -> x0, blocking collectives: 12.8 us -> none  [per_device(): mixed_rows = lax.all_gather(mixed_part, 'tp', axis=1, tiled=True)]
    all_to_all x0 -> x1, waiting for transfers between devices: none -> 7.41 us  [per_device(): lax.all_to_all(jnp.stack([mixed_part] * lax.axis_size('tp')), 'tp', 0, 0)]
    all_to_all x0 -> x1, starting transfers between devices: none -> 3.41 us  [per_device(): lax.all_to_all(jnp.stack([mixed_part] * lax.axis_size('tp')), 'tp', 0, 0)]
    dot_general x1, matrix products: 0.83 us -> 3.03 us  [per_device(): jnp.dot(mixed_rows, out_weight, preferred_element_type=jnp.float32)]
    unnamed x37 -> x45, local copies, waits for them, and re-layouts: 3.58 us -> 5.47 us
  transfers between devices with their start and end apart: 4 -> 5, of which waited for: 4 -> 5; matrix products, arithmetic and copies ran while one was open for 15% -> 15% of each run, Pallas kernels for 0% -> 0%
where the time goes in v1:
time: 141 us; the launch traced here: 140 us
  waiting for transfers between devices  35.2 us (25%)
  blocking collectives  30.2 us (21%)
  local copies, waits for them, and re-layouts  26.3 us (19%)
  starting transfers between devices  19.5 us (14%)
  other arithmetic  14 us (10%)
  matrix products  13.8 us (10%)
    all_to_all x1, blocking collectives, in_one_piece(): lax.all_to_all(both, axis, split_axis=split_dim, concat_axis=concat_dim,...  30.2 us
    all_to_all x1, waiting for transfers between devices, per_device(): lax.all_to_all(partial_rows.reshape(ep_count, per_dev, width).astype(jnp....  11.8 us
    all_to_all x1, waiting for transfers between devices, per_device(): lax.all_to_all(computed, 'ep', split_axis=0, concat_axis=0, tiled=True)  7.67 us
    all_to_all x1, waiting for transfers between devices, per_device(): lax.all_to_all(jnp.stack([mixed_part] * lax.axis_size('tp')), 'tp', 0, 0)  7.41 us
    reduce_sum x1, other arithmetic, per_device(): jnp.sum(jnp.where(is_mine, weights, 0.0)[..., None] * picked, axis=1)  6.28 us
    unnamed x45, local copies, waits for them, and re-layouts  5.47 us
    all_to_all x1, waiting for transfers between devices, sent_and_summed(): lax.all_to_all(in_blocks(array, dim, length), axis, 0, 0, tiled=True)  4.84 us
    convert_element_type x1, local copies, waits for them, and re-layouts, per_device(): picked = flat_back[jnp.where(is_mine, slot_place, 0)].astype(jnp.float32)  4.73 us
  transfers between devices with their start and end apart: 5, of which 5 were waited for; matrix products, arithmetic and copies ran while one was open for 15% of the time, Pallas kernels for 0%

profile of v1, /device:TPU:0, one launch (start us, length us, event | category | flops | bytes accessed | tf_op | source)
XLA Modules:
  0.0 140.1 jit_solution(12846848356802608968)
XLA Ops:
  0.6 1.8 %broadcast_in_dim.22 = bf16[8,128,256]{2,1,0:T(8,128)(2,1)} broadcast(bf16[128,256]{1,0:T(8,128)(2,1)} %param.21), dimensions={1,2} | broadcast | bytes 589824 | tf_op jit(solution)/shard_map/broadcast_in_dim | solution.py:19
  2.5 4.7 %all-to-all-start = ((bf16[8,128,256]{2,1,0:T(8,128)(2,1)}), bf16[8,128,256]{2,1,0:T(8,128)(2,1)S(1)}, u32[]{:S(2)}, u32[]{:S(2)}) async-start(bf16[8,128,256]{2,1,0:T(8,128)(2,1)} %broadcast_in_dim.22), calls=%async_computation | async-start | bytes 1048576 | tf_op jit(solution)/shard_map/all_to_all | solution.py:18
  7.2 0.8 copy.89
  8.1 0.1 eq.50
  8.2 0.7 exp.17
  8.8 0.7 reduce_sum.94
  9.5 0.7 multiply_select_fusion
  10.3 0.1 copy.95
  10.4 0.1 and.23
  10.5 0.1 copy.91
  10.8 0.2 fusion.37
  11.1 0.2 fusion.26
  11.3 0.1 reshape.131
  11.5 1.1 fusion.78
  12.6 0.1 copy.94
  12.8 0.1 copy.86
  13.0 0.8 copy.87
  13.8 0.1 select_reduce_fusion
  14.0 0.1 add_divide_fusion
  14.1 3.4 %all-to-all-done = bf16[8,128,256]{2,1,0:T(8,128)(2,1)S(1)} async-done(((bf16[8,128,256]{2,1,0:T(8,128)(2,1)}), bf16[8,128,256]{2,1,0:T(8,128)(2,1)S(1)}, u32[]{:S(2)}, u32[]{:S(2)}) %all-to-all-start) | async-done | bytes 524320 | tf_op jit(solution)/shard_map/all_to_all | solution.py:18
  17.5 0.8 copy-done.3
  18.5 1.0 copy-done.4
  19.5 0.2 convert_reduce_fusion.1
  19.7 0.4 convolution_convert_fusion.2
  20.2 0.3 fusion.9
  20.5 0.3 fusion.10
  20.8 0.7 copy-done.7
  21.5 0.1 fusion.52
  21.7 0.2 convolution_subtract_fusion
  21.8 0.1 fusion.50
  21.9 0.7 stack.4
  22.7 3.4 %all-to-all-start.1 = ((bf16[8,128,128]{1,2,0:T(8,128)(2,1)}), bf16[8,128,128]{1,2,0:T(8,128)(2,1)S(1)}, u32[]{:S(2)}, u32[]{:S(2)}) async-start(bf16[8,128,128]{1,2,0:T(8,128)(2,1)} %stack.4), calls=%async_computation.1 | async-start | bytes 524288 | tf_op jit(solution)/shard_map/all_to_all | solution.py:144
  26.1 7.4 %all-to-all-done.1 = bf16[8,128,128]{1,2,0:T(8,128)(2,1)S(1)} async-done(((bf16[8,128,128]{1,2,0:T(8,128)(2,1)}), bf16[8,128,128]{1,2,0:T(8,128)(2,1)S(1)}, u32[]{:S(2)}, u32[]{:S(2)}) %all-to-all-start.1) | async-done | bytes 262176 | tf_op jit(solution)/shard_map/all_to_all | solution.py:144
  33.5 3.0 %fusion.75 = (f32[128]{0:T(128)S(1)}, f32[128]{0:T(128)S(1)}, f32[128,2048]{1,0:T(8,128)S(1)}) fusion(f32[128,2048]{1,0:T(8,128)S(1)} %bitcast.120, bf16[128,1024]{0,1:T(8,128)(2,1)S(1)} %bitcast.132, bf16[1024,2048]{1,0:T(8,128)(2,1)} %param.31), kind=kOutput, calls=%fused_computation.127 | convolution fusion | flops 537919232 | bytes 6554624 | tf_op jit(solution)/shard_map/dot_general | solution.py:146
  36.6 1.0 copy-done.2
  37.6 0.2 multiply_convert_fusion
  37.8 0.9 gather_fusion
  38.7 0.1 broadcast_in_dim.32
  38.9 0.2 pad_maximum_fusion
  39.0 30.2 %all_to_all.30 = bf16[16,24,2048]{2,1,0:T(8,128)(2,1)S(1)} all-to-all(bf16[16,24,2048]{2,1,0:T(8,128)(2,1)S(1)} %pad_maximum_fusion), channel_id=1, replica_groups=mesh['ep'=16,'tp'=8] {'ep'}, dimensions={0} | all-to-all | bytes 3145728 | tf_op jit(solution)/shard_map/all_to_all | solution.py:30
  69.3 1.2 copy-done.1
  70.4 0.4 fusion.4
  70.9 3.4 %fusion = bf16[16,8,2048]{2,1,0:T(8,128)(2,1)} fusion(bf16[1,512,2048]{2,1,0:T(8,128)(2,1)S(1)} %copy-done, bf16[1,2048,512]{2,1,0:T(8,128)(2,1)} %param.37, bf16[16,24,2048]{2,1,0:T(8,128)(2,1)} %copy-done.1, f32[128,512]{1,0:T(8,128)S(1)} %fusion.4), kind=kOutput, calls=%fused_computation.6 | convolution fusion | flops 537526272 | bytes 5505024 | tf_op jit(solution)/shard_map/dot_general | solution.py:107
  74.3 3.6 %all-to-all-start.3 = ((bf16[16,8,2048]{2,1,0:T(8,128)(2,1)}), bf16[16,8,2048]{2,1,0:T(8,128)(2,1)S(1)}, u32[]{:S(2)}, u32[]{:S(2)}) async-start(bf16[16,8,2048]{2,1,0:T(8,128)(2,1)} %fusion), calls=%async_computation.3 | async-start | bytes 1048576 | tf_op jit(solution)/shard_map/all_to_all | solution.py:173
  77.9 0.1 copy.88
  78.0 0.1 copy.96
  78.2 2.3 %slice.48 = bf16[16,16,2048]{2,1,0:T(8,128)(2,1)} slice(bf16[16,24,2048]{2,1,0:T(8,128)(2,1)} %copy-done.1), slice={[0:16], [8:24], [0:2048]} | slice | bytes 2097152 | tf_op jit(solution)/shard_map/slice | solution.py:35
  80.5 7.7 %all-to-all-done.3 = bf16[16,8,2048]{2,1,0:T(8,128)(2,1)S(1)} async-done(((bf16[16,8,2048]{2,1,0:T(8,128)(2,1)}), bf16[16,8,2048]{2,1,0:T(8,128)(2,1)S(1)}, u32[]{:S(2)}, u32[]{:S(2)}) %all-to-all-start.3) | async-done | bytes 524320 | tf_op jit(solution)/shard_map/all_to_all | solution.py:173
  88.2 3.3 %gather_fusion.1 = bf16[512,2048]{1,0:T(8,128)(2,1)} fusion(bf16[128,2048]{1,0:T(8,128)(2,1)S(1)} %bitcast.118, s32[1024]{0:T(1024)S(1)} %pad_clamp_fusion), kind=kCustom, calls=%fused_computation.1 | custom fusion | bytes 4196352 | tf_op jit(solution)/shard_map/gather | solution.py:189
  91.5 4.7 %reshape.156 = f32[128,4,2048]{2,1,0:T(4,128)} reshape(bf16[512,2048]{1,0:T(8,128)(2,1)} %gather_fusion.1) | data formatting | bytes 6291456 | tf_op jit(solution)/shard_map/convert_element_type | solution.py:189
  96.3 6.3 %multiply_reduce_fusion = bf16[128,2048]{1,0:T(8,128)(2,1)} fusion(f32[128,4,2048]{2,1,0:T(4,128)} %reshape.156, f32[128,4]{1,0:T(8,128)S(1)} %copy.88), kind=kLoop, calls=%fused_computation.2 | loop fusion | flops 1835008 | bytes 4720640 | tf_op jit(solution)/shard_map/reduce_sum | solution.py:190
  102.5 4.1 %all-to-all-start.4 = ((bf16[8,16,2048]{2,1,0:T(8,128)(2,1)}), bf16[8,16,2048]{2,1,0:T(8,128)(2,1)}, u32[]{:S(2)}, u32[]{:S(2)}) async-start(bf16[8,16,2048]{2,1,0:T(8,128)(2,1)} %bitcast.129), calls=%async_computation.4 | async-start | bytes 1048576 | tf_op jit(solution)/shard_map/all_to_all | solution.py:47
  106.7 1.7 %fusion.79 = f32[256,256]{1,0:T(8,128)S(1)} fusion(bf16[256,2048]{1,0:T(8,128)(2,1)S(1)} %bitcast.121, bf16[2048,256]{1,0:T(8,128)(2,1)} %param.39), kind=kOutput, calls=%fused_computation.129 | convolution fusion | flops 268435456 | bytes 2359296 | tf_op jit(solution)/shard_map/dot_general | solution.py:175
  108.4 3.8 %convolution_convert_fusion = bf16[256,2048]{1,0:T(8,128)(2,1)} fusion(bf16[256,2048]{1,0:T(8,128)(2,1)} %param.41, bf16[256,2048]{1,0:T(8,128)(2,1)S(1)} %bitcast.122, bf16[2048,256]{1,0:T(8,128)(2,1)} %param.40, f32[256,256]{1,0:T(8,128)S(1)} %fusion.79), kind=kOutput, calls=%fused_computation.3 | convolution fusion | flops 537788416 | bytes 4456448 | tf_op jit(solution)/shard_map/dot_general | solution.py:178
  112.2 4.8 %all-to-all-done.4 = bf16[8,16,2048]{2,1,0:T(8,128)(2,1)} async-done(((bf16[8,16,2048]{2,1,0:T(8,128)(2,1)}), bf16[8,16,2048]{2,1,0:T(8,128)(2,1)}, u32[]{:S(2)}, u32[]{:S(2)}) %all-to-all-start.4) | async-done | bytes 524320 | tf_op jit(solution)/shard_map/all_to_all | solution.py:47
  117.0 3.7 %all-to-all-start.5 = ((bf16[16,16,2048]{2,1,0:T(8,128)(2,1)}), bf16[16,16,2048]{2,1,0:T(8,128)(2,1)S(1)}, u32[]{:S(2)}, u32[]{:S(2)}) async-start(bf16[16,16,2048]{2,1,0:T(8,128)(2,1)} %bitcast.133), calls=%async_computation.5 | async-start | bytes 2097152 | tf_op jit(solution)/shard_map/all_to_all | solution.py:179
  120.7 1.8 %copy.98 = f32[1,128,512]{2,1,0:T(8,128)} copy(f32[1,128,512]{1,2,0:T(8,128)} %bitcast.128) | data formatting | bytes 524288 | tf_op jit(solution)/shard_map/stack;reshape | solution.py:90
  122.5 0.8 copy.97
  123.3 1.9 %pad_maximum_fusion.1 = f32[2,128,512]{2,1,0:T(8,128)} fusion(f32[1,128,512]{2,1,0:T(8,128)} %copy.98, f32[1,128,512]{2,1,0:T(8,128)} %copy.97), kind=kLoop, calls=%fused_computation.38 | loop fusion | flops 131072 | bytes 1048576 | tf_op jit(solution)/shard_map/stack | solution.py:90
  125.2 0.1 fusion.18
  125.3 1.1 convert_reduce_fusion.2
  126.4 11.8 %all-to-all-done.5 = bf16[16,16,2048]{2,1,0:T(8,128)(2,1)S(1)} async-done(((bf16[16,16,2048]{2,1,0:T(8,128)(2,1)}), bf16[16,16,2048]{2,1,0:T(8,128)(2,1)S(1)}, u32[]{:S(2)}, u32[]{:S(2)}) %all-to-all-start.5) | async-done | bytes 1048608 | tf_op jit(solution)/shard_map/all_to_all | solution.py:179
  138.3 0.1 convert_reduce_fusion
  138.4 1.6 %add_convert_fusion = bf16[16,2048]{1,0:T(8,128)(2,1)} fusion(f32[16,2048]{1,0:T(8,128)S(1)} %convert_reduce_fusion, f32[16,2048]{1,0:T(8,128)S(1)} %convert_reduce_fusion.2, f32[128,2048]{1,0:T(8,128)} %copy-done.2, s32[]{:T(128)S(6)} %select_n.41, f32[16]{0:T(128)S(1)} %fusion.18), kind=kLoop, calls=%fused_computation.62 | loop fusion | flops 131072 | bytes 458820 | tf_op jit(solution)/shard_map/convert_element_type | solution.py:193
  (59 shorter events, 0.9 us)
Async XLA Ops:
  0.6 70.2 %copy-start = (bf16[1,512,2048]{2,1,0:T(8,128)(2,1)S(1)}, bf16[1,512,2048]{2,1,0:T(8,128)(2,1)}, u32[]{:S(2)}) copy-start(bf16[1,512,2048]{2,1,0:T(8,128)(2,1)} %param.38) | copy-start | bytes 6291460
  2.5 10.1 %copy-start.14 = (s32[128,4]{0,1:T(4,128)S(1)}, s32[128,4]{0,1:T(4,128)}, u32[]{:S(2)}) copy-start(s32[128,4]{0,1:T(4,128)} %param.34) | copy-start | bytes 6148
  2.5 15.0 %all-to-all-start = ((bf16[8,128,256]{2,1,0:T(8,128)(2,1)}), bf16[8,128,256]{2,1,0:T(8,128)(2,1)S(1)}, u32[]{:S(2)}, u32[]{:S(2)}) async-start(bf16[8,128,256]{2,1,0:T(8,128)(2,1)} %broadcast_in_dim.22), calls=%async_computation | async-start | bytes 1048576 | tf_op jit(solution)/shard_map/all_to_all | solution.py:18
  10.6 3.3 %copy-start.17 = (f32[8,64]{1,0:T(8,128)S(1)}, f32[8,64]{1,0:T(8,128)}, u32[]{:S(2)}) copy-start(f32[8,64]{1,0:T(8,128)} %param.26) | copy-start | bytes 6148
  10.6 3.3 %copy-start.18 = (f32[8,64]{1,0:T(8,128)S(1)}, f32[8,64]{1,0:T(8,128)}, u32[]{:S(2)}) copy-start(f32[8,64]{1,0:T(8,128)} %param.25) | copy-start | bytes 6148
  14.1 5.6 %copy-start.15 = (f32[2048]{0:T(1024)S(1)}, f32[2048]{0:T(1024)}, u32[]{:S(2)}) copy-start(f32[2048]{0:T(1024)} %param.22) | copy-start | bytes 24580
  17.5 0.8 copy-start.3
  18.3 1.4 %copy-start.11 = (bf16[2048,128]{1,0:T(8,128)(2,1)S(1)}, bf16[2048,128]{1,0:T(8,128)(2,1)}, u32[]{:S(2)}) copy-start(bf16[2048,128]{1,0:T(8,128)(2,1)} %param.23) | copy-start | bytes 1572868
  18.4 1.1 copy-start.4
  18.4 1.8 %copy-start.6 = (f32[1,128,512]{1,2,0:T(8,128)S(1)}, f32[1,128,512]{1,2,0:T(8,128)}, u32[]{:S(2)}) copy-start(f32[1,128,512]{1,2,0:T(8,128)} %copy.87) | copy-start | bytes 786436
  18.4 1.8 %copy-start.12 = (f32[2,8,64,16]{2,3,1,0:T(8,128)S(1)}, f32[2,8,64,16]{2,3,1,0:T(8,128)}, u32[]{:S(2)}) copy-start(f32[2,8,64,16]{2,3,1,0:T(8,128)} %param.28) | copy-start | bytes 196612
  19.5 2.0 %copy-start.13 = (f32[2,8,16,64]{3,2,1,0:T(8,128)S(1)}, f32[2,8,16,64]{3,2,1,0:T(8,128)}, u32[]{:S(2)}) copy-start(f32[2,8,16,64]{3,2,1,0:T(8,128)} %param.29) | copy-start | bytes 196612
  19.7 2.1 %copy-start.20 = (f32[128]{0:T(128)S(1)}, f32[128]{0:T(128)}, u32[]{:S(2)}) copy-start(f32[128]{0:T(128)} %param.30) | copy-start | bytes 1540
  20.5 1.2 copy-start.9
  20.8 0.7 copy-start.7
  22.7 10.9 %all-to-all-start.1 = ((bf16[8,128,128]{1,2,0:T(8,128)(2,1)}), bf16[8,128,128]{1,2,0:T(8,128)(2,1)S(1)}, u32[]{:S(2)}, u32[]{:S(2)}) async-start(bf16[8,128,128]{1,2,0:T(8,128)(2,1)} %stack.4), calls=%async_computation.1 | async-start | bytes 524288 | tf_op jit(solution)/shard_map/all_to_all | solution.py:144
  33.5 4.0 %copy-start.16 = (f32[2048]{0:T(1024)S(1)}, f32[2048]{0:T(1024)}, u32[]{:S(2)}) copy-start(f32[2048]{0:T(1024)} %param.32) | copy-start | bytes 24580
  36.6 1.0 copy-start.2
  39.0 31.4 %copy-start.10 = (bf16[1,2048,512]{2,1,0:T(8,128)(2,1)S(1)}, bf16[1,2048,512]{2,1,0:T(8,128)(2,1)}, u32[]{:S(2)}) copy-start(bf16[1,2048,512]{2,1,0:T(8,128)(2,1)} %param.36) | copy-start | bytes 6291460
  69.2 1.2 copy-start.1
  74.3 13.9 %all-to-all-start.3 = ((bf16[16,8,2048]{2,1,0:T(8,128)(2,1)}), bf16[16,8,2048]{2,1,0:T(8,128)(2,1)S(1)}, u32[]{:S(2)}, u32[]{:S(2)}) async-start(bf16[16,8,2048]{2,1,0:T(8,128)(2,1)} %fusion), calls=%async_computation.3 | async-start | bytes 1048576 | tf_op jit(solution)/shard_map/all_to_all | solution.py:173
  96.3 10.4 %copy-start.5 = (bf16[16,16,2048]{2,1,0:T(8,128)(2,1)S(1)}, bf16[16,16,2048]{2,1,0:T(8,128)(2,1)}, u32[]{:S(2)}) copy-start(bf16[16,16,2048]{2,1,0:T(8,128)(2,1)} %slice.48) | copy-start | bytes 3145732
  102.5 14.5 %all-to-all-start.4 = ((bf16[8,16,2048]{2,1,0:T(8,128)(2,1)}), bf16[8,16,2048]{2,1,0:T(8,128)(2,1)}, u32[]{:S(2)}, u32[]{:S(2)}) async-start(bf16[8,16,2048]{2,1,0:T(8,128)(2,1)} %bitcast.129), calls=%async_computation.4 | async-start | bytes 1048576 | tf_op jit(solution)/shard_map/all_to_all | solution.py:47
  112.2 8.5 %copy-start.19 = (bf16[2048]{0:T(1024)(128)(2,1)S(1)}, bf16[2048]{0:T(1024)(128)(2,1)}, u32[]{:S(2)}) copy-start(bf16[2048]{0:T(1024)(128)(2,1)} %param.33) | copy-start | bytes 12292
  112.2 10.3 %copy-start.8 = (f32[128,8,64]{0,2,1:T(8,128)S(1)}, f32[128,8,64]{0,2,1:T(8,128)}, u32[]{:S(2)}) copy-start(f32[128,8,64]{0,2,1:T(8,128)} %copy-done.7) | copy-start | bytes 786436
  117.0 21.3 %all-to-all-start.5 = ((bf16[16,16,2048]{2,1,0:T(8,128)(2,1)}), bf16[16,16,2048]{2,1,0:T(8,128)(2,1)S(1)}, u32[]{:S(2)}, u32[]{:S(2)}) async-start(bf16[16,16,2048]{2,1,0:T(8,128)(2,1)} %bitcast.133), calls=%async_computation.5 | async-start | bytes 2097152 | tf_op jit(solution)/shard_map/all_to_all | solution.py:179
